TPU v7x, 256 devices: a whole 4x4x8 slice. The times are simulated.
256 devices in a mesh: fs: 32 (over z, x), tp: 8 (over y, core).
Axes of the slice: x: 4, y: 4, z: 8, core: 2. Of those that a mesh axis runs over, the one named last changes fastest.
Arguments:
- tokens: bfloat16 [32768, 2048], P(('fs', 'tp')), may hold values from -6 to 6
- gate_pre: bfloat16 [32768, 5632], P('fs', 'tp'), may hold values from -6 to 6
- value_pre: bfloat16 [32768, 5632], P('fs', 'tp'), may hold values from -6 to 6
- up_gate_w: bfloat16 [2048, 5632], P('fs', 'tp'), may hold values from -0.078125 to 0.078125
- up_value_w: bfloat16 [2048, 5632], P('fs', 'tp'), may hold values from -0.078125 to 0.078125
- conv_weight: float32 [3, 5632], P(None, 'tp'), may hold values from -3 to 3
- conv_bias: float32 [5632], P('tp'), may hold values from -3 to 3
- hidden_grad: bfloat16 [32768, 5632], P('fs', 'tp'), may hold values from -6 to 6
Outputs:
- input_grad: bfloat16 [32768, 2048], P(('fs', 'tp'))
- up_gate_grad: float32 [2048, 5632], P('fs', 'tp')
- up_value_grad: float32 [2048, 5632], P('fs', 'tp')
- conv_weight_grad: float32 [3, 5632], P(None, 'tp')
- conv_bias_grad: float32 [5632], P('tp')
All inputs are finite; a program needn't handle non-finite values.
Results may differ from a plain program's by a relative error of at most 0.013.
Values may be sent and summed in bfloat16 or wider, within the bound.
No kernel may reach another device: no remote copies, remote signals or barrier semaphores. Data moves between devices by JAX's collectives and lax.ppermute only.
A program may use at most 128 MiB of HBM per device.

v0:
```python
import jax
import jax.numpy as jnp
from jax import lax
from jax.sharding import Mesh
from jax.sharding import PartitionSpec as P

FS = ("fs_0", "fs_1")
FS_TP = ("fs_0", "fs_1", "tp")


def copy_for_each(shard, axis):
    peers = lax.axis_size(axis)
    return lax.all_to_all(
        jnp.broadcast_to(shard[None], (peers, *shard.shape)), axis, 0, 0, tiled=True
    )


def taken_together(shard, axis):
    return copy_for_each(shard, axis).sum(axis=0)


def in_one_piece(arrays, axis, dim, along):
    ends, at = ([], 0)
    for a in arrays[:-1]:
        at += a.shape[along]
        ends.append(at)
    both = jnp.concatenate(arrays, axis=along)
    return tuple(jnp.split(lax.all_gather(both, axis, axis=dim, tiled=True), ends, axis=along))


def summed_rows(subtotal, axes):
    for axis in axes:
        subtotal = lax.psum_scatter(subtotal, axis, scatter_dimension=0, tiled=True)
    return subtotal


def in_blocks(shard, dim, peers):
    lengths = shard.shape
    blocks = shard.reshape(*lengths[:dim], peers, lengths[dim] // peers, *lengths[dim + 1 :])
    return jnp.moveaxis(blocks, dim, 0)


def summed_on_arrival(shard, axis, dim):
    blocks = in_blocks(shard, dim, lax.axis_size(axis))
    arrived = lax.all_to_all(blocks, axis, split_axis=0, concat_axis=0, tiled=True)
    return arrived.astype(jnp.float32).sum(axis=0)


def contract_rows(left, right):
    return lax.dot_general(
        left, right, (((0,), (0,)), ((), ())), preferred_element_type=jnp.float32
    )


def contract_cols(left, right):
    return lax.dot_general(
        left, right, (((1,), (1,)), ((), ())), preferred_element_type=jnp.float32
    )


def on_device(
    tokens, gate_pre, value_pre, up_gate_w, up_value_w, conv_weight, conv_bias, hidden_grad
):
    length = gate_pre.shape[0]
    col_count = gate_pre.shape[1]
    scale = float(length * lax.axis_size(FS)) ** (-0.5)
    gate_float = gate_pre.astype(jnp.float32)
    padded = jnp.pad(gate_float, ((2, 0), (0, 0)))
    gate_conv = (
        conv_bias
        + conv_weight[0] * padded[:length]
        + conv_weight[1] * padded[1 : length + 1]
        + conv_weight[2] * padded[2:]
    )
    active, gelu_back = jax.vjp(jax.nn.gelu, gate_conv)
    grad_float = hidden_grad.astype(jnp.float32)
    value_grad = (grad_float * active).astype(jnp.bfloat16)
    conv_grad = gelu_back(grad_float * value_pre.astype(jnp.float32))[0]
    shifted = jnp.pad(conv_grad, ((0, 2), (0, 0)))
    gate_grad = (
        conv_weight[2] * conv_grad
        + conv_weight[1] * shifted[1 : length + 1]
        + conv_weight[0] * shifted[2:]
    ).astype(jnp.bfloat16)
    conv_terms = jnp.stack(
        [
            jnp.sum(conv_grad * padded[:length], axis=0),
            jnp.sum(conv_grad * padded[1 : length + 1], axis=0),
            jnp.sum(conv_grad * padded[2:], axis=0),
            jnp.sum(conv_grad, axis=0),
        ]
    )
    conv_total = taken_together(conv_terms, FS) * scale
    whole_tokens = lax.all_gather(tokens, "tp", axis=0, tiled=True)
    full_gate, full_value = in_one_piece((up_gate_w, up_value_w), FS, 0, 1)
    joined = summed_rows(
        jnp.concatenate(
            [contract_rows(whole_tokens, gate_grad), contract_rows(whole_tokens, value_grad)],
            axis=1,
        ),
        FS,
    )
    gate_out = joined[:, :col_count] * scale
    value_out = joined[:, col_count:] * scale
    input_grad = summed_on_arrival(
        (contract_cols(gate_grad, full_gate) + contract_cols(value_grad, full_value)).astype(
            jnp.bfloat16
        ),
        "tp",
        0,
    ).astype(jnp.bfloat16)
    return (input_grad, gate_out, value_out, conv_total[:3], conv_total[3])


def solution(mesh):
    finer = Mesh(mesh.devices.reshape(8, 4, mesh.shape["tp"]), ("fs_0", "fs_1", "tp"))
    in_specs = (
        P(FS_TP, None),
        P(FS, "tp"),
        P(FS, "tp"),
        P(FS, "tp"),
        P(FS, "tp"),
        P(None, "tp"),
        P("tp"),
        P(FS, "tp"),
    )
    out_specs = (P(FS_TP, None), P(FS, "tp"), P(FS, "tp"), P(None, "tp"), P("tp"))
    return jax.shard_map(
        on_device, mesh=finer, in_specs=in_specs, out_specs=out_specs, check_vma=False
    )
```

profile of v0, /device:TPU:8, one launch (start us, length us, event | category | flops | bytes accessed | tf_op | source)
XLA Modules:
  0.0 301.7 jit_solution(17411305977214108581)
XLA Ops:
  7.2 0.0 copy-start
  7.2 0.0 copy-start.7
  7.2 0.0 copy-start.2
  7.2 0.0 copy-start.8
  7.2 0.0 all-gather.5.cloned.1.call-start
  7.3 0.7 all-gather.5.cloned.1.call-update
  7.9 0.0 all-gather.3.cloned.1.call-start
  8.0 1.8 pad_maximum_fusion.1
  9.8 0.0 all-gather.3.cloned.1.call-update
  9.8 0.0 reduce-scatter.5.cloned.1.call-start
  9.9 0.0 copy-start.3
  9.9 1.8 convert_element_type.26
  11.7 0.0 copy-done.7
  11.8 0.0 copy-done
  11.8 0.0 copy-done.2
  11.8 0.0 copy-done.8
  11.8 0.0 copy-done.3
  11.8 6.5 %multiply_reduce_fusion.2 = (f32[704]{0:T(1024)S(1)}, f32[704]{0:T(1024)S(1)}, f32[704]{0:T(1024)S(1)}, f32[704]{0:T(1024)S(1)}, f32[1024,704]{0,1:T(8,128)S(1)}, /*index=5*/f32[1024,704]{0,1:T(8,128)}) fusion(f32[1024,704]{0,1:T(8,128)S(1)} %convert_element_type.26, bf16[1024,704]{0,1:T(8,128)(2,1)S(1)} %copy-done, bf16[1024,704]{0,1:T(8,128)(2,1)S(1)} %copy-done.2, ...), kind=kLoop, calls=%fused_computation.29 | loop fusion | flops 25949440 | bytes 12998656 | tf_op jit(solution)/shard_map/reduce_sum | solution.py:87
  18.3 3.0 %fusion.6 = bf16[1024,704]{0,1:T(8,128)(2,1)} fusion(f32[1024,704]{0,1:T(8,128)S(1)} %get-tuple-element.32, f32[704]{0:T(1024)S(1)} %get-tuple-element.30, f32[704]{0:T(1024)S(1)} %get-tuple-element.31, f32[704]{0:T(1024)S(1)} %get-tuple-element.29), kind=kLoop, calls=%fused_computation.18 | loop fusion | flops 4325376 | bytes 4333824 | tf_op jit(solution)/shard_map/convert_element_type | solution.py:84
  21.4 25.0 %all-gather.5.cloned.1.call-done = bf16[1024,2048]{1,0:T(8,128)(2,1)} async-done(((bf16[128,2048]{1,0:T(8,128)(2,1)}), bf16[1024,2048]{1,0:T(8,128)(2,1)}) %all-gather.5.cloned.1.call-update) | async-done | bytes 4194320 | tf_op jit(solution)/shard_map/all_gather | solution.py:94
  46.4 8.4 %convolution_bitcast_fusion.1 = f32[2048,704]{0,1:T(8,128)} fusion(bf16[1024,704]{0,1:T(8,128)(2,1)} %fusion.6, bf16[1024,2048]{1,0:T(8,128)(2,1)} %all-gather.5.cloned.1.call-done), kind=kOutput, calls=%fused_computation.5 | convolution fusion | flops 2952790016 | bytes 11403264 | tf_op jit(solution)/shard_map/dot_general | solution.py:50
  54.8 0.0 copy-done.1
  54.8 0.0 copy-done.10
  54.8 5.3 %convolution_bitcast_fusion = f32[2048,704]{0,1:T(8,128)} fusion(bf16[1024,2048]{1,0:T(8,128)(2,1)S(1)} %copy-done.10, bf16[1024,704]{0,1:T(8,128)(2,1)S(1)} %copy-done.4, f32[1024,704]{0,1:T(8,128)S(1)} %copy-done.1), kind=kOutput, calls=%fused_computation.4 | convolution fusion | flops 2960719872 | bytes 14286848 | tf_op jit(solution)/shard_map/dot_general | solution.py:50
  60.1 10.8 %pad_maximum_fusion = f32[2048,1408]{0,1:T(8,128)} fusion(f32[2048,704]{0,1:T(8,128)} %convolution_bitcast_fusion, f32[2048,704]{0,1:T(8,128)} %convolution_bitcast_fusion.1), kind=kLoop, calls=%fused_computation | loop fusion | flops 2883584 | bytes 23068672 | tf_op jit(solution)/shard_map/concatenate | solution.py:97
  70.9 0.0 reduce-scatter.5.cloned.1.call-update
  71.0 0.8 broadcast_in_dim.2
  71.8 10.0 %all-to-all-start.1 = ((f32[32,4,704]{2,1,0:T(4,128)}), f32[32,4,704]{2,1,0:T(4,128)S(1)}, u32[]{:S(2)}, u32[]{:S(2)}) async-start(f32[32,4,704]{2,1,0:T(4,128)} %broadcast_in_dim.2), calls=%async_computation.2 | async-start | bytes 786432 | tf_op jit(solution)/shard_map/all_to_all | solution.py:13
  81.8 56.8 %all-gather.3.cloned.1.call-done = bf16[2048,1408]{1,0:T(8,128)(2,1)} async-done(((bf16[64,1408]{1,0:T(8,128)(2,1)}), bf16[2048,1408]{1,0:T(8,128)(2,1)}) %all-gather.3.cloned.1.call-update) | async-done | bytes 5767184 | tf_op jit(solution)/shard_map/all_gather | solution.py:28
  138.7 6.0 %fusion.1 = f32[1024,2048]{1,0:T(8,128)S(1)} fusion(bf16[1024,704]{0,1:T(8,128)(2,1)} %fusion.6, bf16[2048,1408]{1,0:T(8,128)(2,1)} %all-gather.3.cloned.1.call-done), kind=kOutput, calls=%fused_computation.13 | convolution fusion | flops 2952790016 | bytes 12976128 | tf_op jit(solution)/shard_map/dot_general | solution.py:56
  144.7 7.6 %add_convert_fusion = bf16[1024,2048]{1,0:T(8,128)(2,1)} fusion(f32[1024,2048]{1,0:T(8,128)S(1)} %fusion.1, bf16[2048,1408]{1,0:T(8,128)(2,1)S(1)} %copy-done.9, bf16[1024,704]{0,1:T(8,128)(2,1)S(1)} %copy-done.5, f32[1024,704]{0,1:T(8,128)S(1)} %copy-done.1), kind=kOutput, calls=%fused_computation.1 | convolution fusion | flops 2964914176 | bytes 20054016 | tf_op jit(solution)/shard_map/dot_general | solution.py:56
  152.3 0.0 all-to-all-done.1
  152.3 5.0 %all-to-all-start = ((bf16[8,128,2048]{2,1,0:T(8,128)(2,1)}), bf16[8,128,2048]{2,1,0:T(8,128)(2,1)}, u32[]{:S(2)}, u32[]{:S(2)}) async-start(bf16[8,128,2048]{2,1,0:T(8,128)(2,1)} %bitcast.11), calls=%async_computation | async-start | bytes 8388608 | tf_op jit(solution)/shard_map/all_to_all | solution.py:45
  157.3 0.0 reduce-scatter.7.cloned.1.call-start
  157.3 105.4 %reduce-scatter.5.cloned.1.call-done = f32[256,1408]{0,1:T(8,128)} async-done(((f32[2048,1408]{0,1:T(8,128)}), f32[256,1408]{0,1:T(8,128)}) %reduce-scatter.5.cloned.1.call-update) | async-done | bytes 1441808 | tf_op jit(solution)/shard_map/reduce_scatter | solution.py:33
  262.6 2.9 copy.22
  265.5 0.0 reduce-scatter.7.cloned.1.call-update
  265.6 0.1 reduce_sum.62
  265.7 0.0 copy-start.6
  265.7 0.6 slice_reduce_fusion
  266.3 0.0 all-to-all-done
  266.3 3.8 %reduce_sum.57 = bf16[128,2048]{1,0:T(8,128)(2,1)} reduce(bf16[8,128,2048]{2,1,0:T(8,128)(2,1)} %all-to-all-done, bf16[]{:T(256)} %constant.19.clone.1), dimensions={0}, to_apply=%region_0.1 | reduce | flops 1835008 | bytes 4718594 | tf_op jit(solution)/shard_map/reduce_sum | solution.py:46
  270.1 21.8 %reduce-scatter.7.cloned.1.call-done = f32[64,1408]{1,0:T(8,128)} async-done(((f32[256,1408]{1,0:T(8,128)}), f32[64,1408]{1,0:T(8,128)}) %reduce-scatter.7.cloned.1.call-update) | async-done | bytes 360464
  292.0 1.1 fusion.18
  293.1 0.2 copy.25
  293.3 0.8 copy.20
  294.1 0.2 copy.26
  294.3 0.8 copy.21
  (18 shorter events, 0.2 us)
Async XLA Ops:
  7.2 4.6 %copy-start = (bf16[1024,704]{0,1:T(8,128)(2,1)S(1)}, bf16[1024,704]{0,1:T(8,128)(2,1)}, u32[]{:S(2)}) copy-start(bf16[1024,704]{0,1:T(8,128)(2,1)} %param.9) | copy-start | bytes 4325380
  7.2 4.5 %copy-start.7 = (f32[3,704]{1,0:T(4,128)S(1)}, f32[3,704]{1,0:T(4,128)}, u32[]{:S(2)}) copy-start(f32[3,704]{1,0:T(4,128)} %param.13) | copy-start | bytes 25348
  7.2 4.6 %copy-start.2 = (bf16[1024,704]{0,1:T(8,128)(2,1)S(1)}, bf16[1024,704]{0,1:T(8,128)(2,1)}, u32[]{:S(2)}) copy-start(bf16[1024,704]{0,1:T(8,128)(2,1)} %param.10) | copy-start | bytes 4325380
  7.2 4.6 %copy-start.8 = (f32[704]{0:T(1024)S(1)}, f32[704]{0:T(1024)}, u32[]{:S(2)}) copy-start(f32[704]{0:T(1024)} %param.14) | copy-start | bytes 8452
  7.2 39.2 %all-gather.5.cloned.1.call-start = ((), (), s32[]{:S(2)}) async-start(), calls=%async_computation.5 | async-start | bytes 4718592 | tf_op jit(solution)/shard_map/all_gather | solution.py:94
  7.9 130.7 %all-gather.3.cloned.1.call-start = ((), (), s32[]{:S(2)}) async-start(), calls=%async_computation.4 | async-start | bytes 5947392 | tf_op jit(solution)/shard_map/all_gather | solution.py:28
  9.8 252.8 %reduce-scatter.5.cloned.1.call-start = ((), (), s32[]{:S(2)}) async-start(), calls=%async_computation.6 | async-start | bytes 12976128 | tf_op jit(solution)/shard_map/reduce_scatter | solution.py:33
  9.9 1.9 copy-start.3
  21.4 33.4 %copy-start.1 = (f32[1024,704]{0,1:T(8,128)S(1)}, f32[1024,704]{0,1:T(8,128)}, u32[]{:S(2)}) copy-start(f32[1024,704]{0,1:T(8,128)} %get-tuple-element.33) | copy-start | bytes 8650756
  46.4 8.4 %copy-start.4 = (bf16[1024,704]{0,1:T(8,128)(2,1)S(1)}, bf16[1024,704]{0,1:T(8,128)(2,1)}, u32[]{:S(2)}) copy-start(bf16[1024,704]{0,1:T(8,128)(2,1)} %param.15) | copy-start | bytes 4325380
  46.4 8.4 %copy-start.10 = (bf16[1024,2048]{1,0:T(8,128)(2,1)S(1)}, bf16[1024,2048]{1,0:T(8,128)(2,1)}, u32[]{:S(2)}) copy-start(bf16[1024,2048]{1,0:T(8,128)(2,1)} %all-gather.5.cloned.1.call-done) | copy-start | bytes 12582916
  71.8 80.4 %all-to-all-start.1 = ((f32[32,4,704]{2,1,0:T(4,128)}), f32[32,4,704]{2,1,0:T(4,128)S(1)}, u32[]{:S(2)}, u32[]{:S(2)}) async-start(f32[32,4,704]{2,1,0:T(4,128)} %broadcast_in_dim.2), calls=%async_computation.2 | async-start | bytes 786432 | tf_op jit(solution)/shard_map/all_to_all | solution.py:13
  138.7 6.0 %copy-start.5 = (bf16[1024,704]{0,1:T(8,128)(2,1)S(1)}, bf16[1024,704]{0,1:T(8,128)(2,1)}, u32[]{:S(2)}) copy-start(bf16[1024,704]{0,1:T(8,128)(2,1)} %param.15) | copy-start | bytes 4325380
  138.7 6.0 %copy-start.9 = (bf16[2048,1408]{1,0:T(8,128)(2,1)S(1)}, bf16[2048,1408]{1,0:T(8,128)(2,1)}, u32[]{:S(2)}) copy-start(bf16[2048,1408]{1,0:T(8,128)(2,1)} %all-gather.3.cloned.1.call-done) | copy-start | bytes 17301508
  152.3 114.0 %all-to-all-start = ((bf16[8,128,2048]{2,1,0:T(8,128)(2,1)}), bf16[8,128,2048]{2,1,0:T(8,128)(2,1)}, u32[]{:S(2)}, u32[]{:S(2)}) async-start(bf16[8,128,2048]{2,1,0:T(8,128)(2,1)} %bitcast.11), calls=%async_computation | async-start | bytes 8388608 | tf_op jit(solution)/shard_map/all_to_all | solution.py:45
  157.3 134.7 %reduce-scatter.7.cloned.1.call-start = ((), (), s32[]{:S(2)}) async-start(), calls=%async_computation.7 | async-start | bytes 1802240
  265.7 27.6 %copy-start.6 = (f32[4,704]{1,0:T(4,128)}, f32[4,704]{1,0:T(4,128)S(1)}, u32[]{:S(2)}) copy-start(f32[4,704]{1,0:T(4,128)S(1)} %broadcast_multiply_fusion.2) | copy-start | bytes 33796
Sparse Core Ops, SparseCore 0:
  9.9 36.4 all-gather.4
  49.5 89.0 all-gather.2
  141.2 121.3 reduce-scatter.4
  265.7 26.2 reduce-scatter.6
where the time goes:
time: 302 us
  waiting for transfers between devices  210 us (70%)
  other arithmetic  28 us (9%)
  matrix products  27.3 us (9%)
  starting transfers between devices  15.1 us (5%)
  between operations  14 us (5%)
  local copies, waits for them, and re-layouts  7.54 us (2%)
    reduce_scatter x1, waiting for transfers between devices, summed_rows(): subtotal = lax.psum_scatter(subtotal, axis, scatter_dimension=0, tiled=True)  105 us
    all_gather x1, waiting for transfers between devices, in_one_piece(): lax.all_gather(both, axis, axis=dim, tiled=True)  56.8 us
    all_gather x1, waiting for transfers between devices, on_device(): whole_tokens = lax.all_gather(tokens, 'tp', axis=0, tiled=True)  25 us
    unnamed x5, waiting for transfers between devices  22.5 us
    dot_general x2, matrix products, contract_rows(): lax.dot_general(left, right, (((0,), (0,)), ((), ())), preferred_element_...  13.7 us
    dot_general x2, matrix products, contract_cols(): lax.dot_general(left, right, (((1,), (1,)), ((), ())), preferred_element_...  13.6 us
    concatenate x1, other arithmetic, on_device(): jnp.concatenate([contract_rows(whole_tokens, gate_grad), contract_rows(wh...  10.8 us
    all_to_all x1, starting transfers between devices, copy_for_each(): lax.all_to_all(jnp.broadcast_to(shard[None], (peers, *shard.shape)), axis...  10 us
  transfers between devices with their start and end apart: 6, of which 4 were waited for; matrix products, arithmetic and copies ran while one was open for 20% of the time, Pallas kernels for 0%

commit v1 on v0

--- a/solution.py
+++ b/solution.py
@@ -91,7 +91,9 @@
         ]
     )
     conv_total = taken_together(conv_terms, FS) * scale
-    whole_tokens = lax.all_gather(tokens, "tp", axis=0, tiled=True)
+    whole_tokens = jnp.concatenate(
+        lax.all_to_all(jnp.stack([tokens for _ in range(lax.axis_size("tp"))]), "tp", 0, 0), axis=0
+    )
     full_gate, full_value = in_one_piece((up_gate_w, up_value_w), FS, 0, 1)
     joined = summed_rows(
         jnp.concatenate(

time: 302 us -> 267 us (0.88)
  waiting for transfers between devices: 210 us -> 158 us
  starting transfers between devices: 15.1 us -> 23 us
  local copies, waits for them, and re-layouts: 7.54 us -> 12.4 us
  matrix products: 27.3 us -> 30.5 us
    all_gather x1, waiting for transfers between devices: 56.8 us -> 0.02 us  [in_one_piece(): lax.all_gather(both, axis, axis=dim, tiled=True)]
    all_to_all x0 -> x1, waiting for transfers between devices: none -> 36.9 us  [on_device(): lax.all_to_all(jnp.stack([tokens for _ in range(lax.axis_size('tp'))]), '...]
    all_gather x1 -> x0, waiting for transfers between devices: 25 us -> none  [on_device(): whole_tokens = lax.all_gather(tokens, 'tp', axis=0, tiled=True)]
    reduce_scatter x1, waiting for transfers between devices: 105 us -> 95.6 us  [summed_rows(): subtotal = lax.psum_scatter(subtotal, axis, scatter_dimension=0, tiled=True)]
    all_to_all x0 -> x1, starting transfers between devices: none -> 6.71 us  [on_device(): lax.all_to_all(jnp.stack([tokens for _ in range(lax.axis_size('tp'))]), '...]
    all_to_all x1, waiting for transfers between devices: 0.01 us -> 4.28 us  [copy_for_each(): lax.all_to_all(jnp.broadcast_to(shard[None], (peers, *shard.shape)), axis...]
    another operation x0 -> x1, local copies, waits for them, and re-layouts: none -> 3.54 us  [on_device(): jnp.stack([tokens for _ in range(lax.axis_size('tp'))])]
    unnamed x5 -> x4, waiting for transfers between devices: 22.5 us -> 21 us
  transfers between devices with their start and end apart: 6 -> 6, of which waited for: 4 -> 4; matrix products, arithmetic and copies ran while one was open for 20% -> 24% of each run, Pallas kernels for 0% -> 0%
where the time goes in v1:
time: 267 us; the launch traced here: 266 us
  waiting for transfers between devices  158 us (59%)
  matrix products  30.5 us (11%)
  other arithmetic  26.4 us (10%)
  starting transfers between devices  23 us (9%)
  between operations  15.7 us (6%)
  local copies, waits for them, and re-layouts  12.4 us (5%)
    reduce_scatter x1, waiting for transfers between devices, summed_rows(): subtotal = lax.psum_scatter(subtotal, axis, scatter_dimension=0, tiled=True)  95.6 us
    all_to_all x1, waiting for transfers between devices, on_device(): lax.all_to_all(jnp.stack([tokens for _ in range(lax.axis_size('tp'))]), '...  36.9 us
    unnamed x4, waiting for transfers between devices  21 us
    dot_general x2, matrix products, contract_rows(): lax.dot_general(left, right, (((0,), (0,)), ((), ())), preferred_element_...  16 us
    dot_general x2, matrix products, contract_cols(): lax.dot_general(left, right, (((1,), (1,)), ((), ())), preferred_element_...  14.6 us
    concatenate x1, other arithmetic, on_device(): jnp.concatenate([contract_rows(whole_tokens, gate_grad), contract_rows(wh...  10.8 us
    all_to_all x1, starting transfers between devices, copy_for_each(): lax.all_to_all(jnp.broadcast_to(shard[None], (peers, *shard.shape)), axis...  9.75 us
    all_to_all x1, starting transfers between devices, on_device(): lax.all_to_all(jnp.stack([tokens for _ in range(lax.axis_size('tp'))]), '...  6.71 us
  transfers between devices with their start and end apart: 6, of which 4 were waited for; matrix products, arithmetic and copies ran while one was open for 24% of the time, Pallas kernels for 0%

profile of v1, /device:TPU:8, one launch (start us, length us, event | category | flops | bytes accessed | tf_op | source)
XLA Modules:
  0.0 266.0 jit_solution(5725598318120674281)
XLA Ops:
  8.0 0.0 all-gather.2.cloned.1.call-start
  8.0 1.7 pad_maximum_fusion.1
  9.8 0.0 all-gather.2.cloned.1.call-update
  9.8 3.5 %stack.12 = bf16[8,128,2048]{2,1,0:T(8,128)(2,1)} broadcast(bf16[128,2048]{1,0:T(8,128)(2,1)} %param.8), dimensions={1,2} | broadcast | bytes 4718592 | tf_op jit(solution)/shard_map/stack | solution.py:95
  13.3 6.7 %all-to-all-start.1 = ((bf16[8,128,2048]{2,1,0:T(8,128)(2,1)}), bf16[8,128,2048]{2,1,0:T(8,128)(2,1)}, u32[]{:S(2)}, u32[]{:S(2)}) async-start(bf16[8,128,2048]{2,1,0:T(8,128)(2,1)} %stack.12), calls=%async_computation.1 | async-start | bytes 8388608 | tf_op jit(solution)/shard_map/all_to_all | solution.py:95
  20.0 0.0 reduce-scatter.5.cloned.1.call-start
  20.1 0.0 copy-done
  20.1 0.0 copy-start.3
  20.1 0.4 convert_element_type.26
  20.5 0.2 copy-done.7
  20.8 0.6 copy-done.2
  21.4 0.0 copy-done.8
  21.4 0.5 copy-done.3
  21.9 6.5 %multiply_reduce_fusion.2 = (f32[704]{0:T(1024)S(1)}, f32[704]{0:T(1024)S(1)}, f32[704]{0:T(1024)S(1)}, f32[704]{0:T(1024)S(1)}, f32[1024,704]{0,1:T(8,128)S(1)}, /*index=5*/f32[1024,704]{0,1:T(8,128)}) fusion(f32[1024,704]{0,1:T(8,128)S(1)} %convert_element_type.26, bf16[1024,704]{0,1:T(8,128)(2,1)S(1)} %copy-done, bf16[1024,704]{0,1:T(8,128)(2,1)S(1)} %copy-done.2, ...), kind=kLoop, calls=%fused_computation.29 | loop fusion | flops 25949440 | bytes 12998656 | tf_op jit(solution)/shard_map/reduce_sum | solution.py:87
  28.4 3.0 %fusion.6 = bf16[1024,704]{0,1:T(8,128)(2,1)} fusion(f32[1024,704]{0,1:T(8,128)S(1)} %get-tuple-element.32, f32[704]{0:T(1024)S(1)} %get-tuple-element.30, f32[704]{0:T(1024)S(1)} %get-tuple-element.31, f32[704]{0:T(1024)S(1)} %get-tuple-element.29), kind=kLoop, calls=%fused_computation.18 | loop fusion | flops 4325376 | bytes 4333824 | tf_op jit(solution)/shard_map/convert_element_type | solution.py:84
  31.4 36.9 %all-to-all-done.1 = bf16[8,128,2048]{2,1,0:T(8,128)(2,1)} async-done(((bf16[8,128,2048]{2,1,0:T(8,128)(2,1)}), bf16[8,128,2048]{2,1,0:T(8,128)(2,1)}, u32[]{:S(2)}, u32[]{:S(2)}) %all-to-all-start.1) | async-done | bytes 4194336 | tf_op jit(solution)/shard_map/all_to_all | solution.py:95
  68.4 8.4 %convolution_bitcast_fusion.1 = f32[2048,704]{0,1:T(8,128)} fusion(bf16[1024,704]{0,1:T(8,128)(2,1)} %fusion.6, bf16[1024,2048]{1,0:T(8,128)(2,1)} %bitcast.1), kind=kOutput, calls=%fused_computation.5 | convolution fusion | flops 2952790016 | bytes 11403264 | tf_op jit(solution)/shard_map/dot_general | solution.py:50
  76.8 0.0 copy-done.1
  76.8 0.0 copy-done.4
  76.8 7.5 %convolution_bitcast_fusion = f32[2048,704]{0,1:T(8,128)} fusion(bf16[1024,2048]{1,0:T(8,128)(2,1)} %bitcast.1, bf16[1024,704]{0,1:T(8,128)(2,1)S(1)} %copy-done.4, f32[1024,704]{0,1:T(8,128)S(1)} %copy-done.1), kind=kOutput, calls=%fused_computation.4 | convolution fusion | flops 2960719872 | bytes 14286848 | tf_op jit(solution)/shard_map/dot_general | solution.py:50
  84.3 10.8 %pad_maximum_fusion = f32[2048,1408]{0,1:T(8,128)} fusion(f32[2048,704]{0,1:T(8,128)} %convolution_bitcast_fusion, f32[2048,704]{0,1:T(8,128)} %convolution_bitcast_fusion.1), kind=kLoop, calls=%fused_computation | loop fusion | flops 2883584 | bytes 23068672 | tf_op jit(solution)/shard_map/concatenate | solution.py:99
  95.1 0.0 reduce-scatter.5.cloned.1.call-update
  95.2 0.8 broadcast_in_dim.2
  96.0 9.8 %all-to-all-start.2 = ((f32[32,4,704]{2,1,0:T(4,128)}), f32[32,4,704]{2,1,0:T(4,128)S(1)}, u32[]{:S(2)}, u32[]{:S(2)}) async-start(f32[32,4,704]{2,1,0:T(4,128)} %broadcast_in_dim.2), calls=%async_computation.3 | async-start | bytes 786432 | tf_op jit(solution)/shard_map/all_to_all | solution.py:13
  105.8 0.0 all-gather.2.cloned.1.call-done
  105.8 0.0 copy-start.5
  105.8 0.0 copy-start.9
  105.8 7.0 %fusion.1 = f32[1024,2048]{1,0:T(8,128)S(1)} fusion(bf16[1024,704]{0,1:T(8,128)(2,1)} %fusion.6, bf16[2048,1408]{1,0:T(8,128)(2,1)} %all-gather.2.cloned.1.call-done), kind=kOutput, calls=%fused_computation.13 | convolution fusion | flops 2952790016 | bytes 12976128 | tf_op jit(solution)/shard_map/dot_general | solution.py:56
  112.8 0.0 copy-done.5
  112.8 0.0 copy-done.9
  112.8 7.6 %add_convert_fusion = bf16[1024,2048]{1,0:T(8,128)(2,1)} fusion(f32[1024,2048]{1,0:T(8,128)S(1)} %fusion.1, bf16[2048,1408]{1,0:T(8,128)(2,1)S(1)} %copy-done.9, bf16[1024,704]{0,1:T(8,128)(2,1)S(1)} %copy-done.5, f32[1024,704]{0,1:T(8,128)S(1)} %copy-done.1), kind=kOutput, calls=%fused_computation.1 | convolution fusion | flops 2964914176 | bytes 20054016 | tf_op jit(solution)/shard_map/dot_general | solution.py:56
  120.4 4.3 %all-to-all-done.2 = f32[32,4,704]{2,1,0:T(4,128)S(1)} async-done(((f32[32,4,704]{2,1,0:T(4,128)}), f32[32,4,704]{2,1,0:T(4,128)S(1)}, u32[]{:S(2)}, u32[]{:S(2)}) %all-to-all-start.2) | async-done | bytes 360480 | tf_op jit(solution)/shard_map/all_to_all | solution.py:13
  124.7 6.5 %all-to-all-start = ((bf16[8,128,2048]{2,1,0:T(8,128)(2,1)}), bf16[8,128,2048]{2,1,0:T(8,128)(2,1)}, u32[]{:S(2)}, u32[]{:S(2)}) async-start(bf16[8,128,2048]{2,1,0:T(8,128)(2,1)} %bitcast.12), calls=%async_computation | async-start | bytes 8388608 | tf_op jit(solution)/shard_map/all_to_all | solution.py:45
  131.2 0.0 reduce-scatter.7.cloned.1.call-start
  131.2 95.6 %reduce-scatter.5.cloned.1.call-done = f32[256,1408]{0,1:T(8,128)} async-done(((f32[2048,1408]{0,1:T(8,128)}), f32[256,1408]{0,1:T(8,128)}) %reduce-scatter.5.cloned.1.call-update) | async-done | bytes 1441808 | tf_op jit(solution)/shard_map/reduce_scatter | solution.py:33
  226.8 2.9 %copy.22 = f32[256,1408]{1,0:T(8,128)} copy(f32[256,1408]{0,1:T(8,128)} %reduce-scatter.5.cloned.1.call-done) | data formatting | bytes 2883584
  229.8 0.0 reduce-scatter.7.cloned.1.call-update
  229.8 0.1 reduce_sum.62
  229.9 0.0 copy-start.6
  229.9 0.6 slice_reduce_fusion
  230.5 0.0 all-to-all-done
  230.5 3.8 %reduce_sum.57 = bf16[128,2048]{1,0:T(8,128)(2,1)} reduce(bf16[8,128,2048]{2,1,0:T(8,128)(2,1)} %all-to-all-done, bf16[]{:T(256)} %constant.19.clone.1), dimensions={0}, to_apply=%region_0.1 | reduce | flops 1835008 | bytes 4718594 | tf_op jit(solution)/shard_map/reduce_sum | solution.py:46
  234.3 21.0 %reduce-scatter.7.cloned.1.call-done = f32[64,1408]{1,0:T(8,128)} async-done(((f32[256,1408]{1,0:T(8,128)}), f32[64,1408]{1,0:T(8,128)}) %reduce-scatter.7.cloned.1.call-update) | async-done | bytes 360464
  255.3 1.1 fusion.18
  256.4 0.2 copy.25
  256.7 0.8 copy.20
  257.5 0.2 copy.26
  257.7 0.8 copy.21
  (16 shorter events, 0.2 us)
Async XLA Ops:
  8.0 97.8 %all-gather.2.cloned.1.call-start = ((), (), s32[]{:S(2)}) async-start(), calls=%async_computation.5 | async-start | bytes 5947392 | tf_op jit(solution)/shard_map/all_gather | solution.py:28
  13.3 6.8 %copy-start = (bf16[1024,704]{0,1:T(8,128)(2,1)S(1)}, bf16[1024,704]{0,1:T(8,128)(2,1)}, u32[]{:S(2)}) copy-start(bf16[1024,704]{0,1:T(8,128)(2,1)} %param.9) | copy-start | bytes 4325380
  13.3 55.0 %all-to-all-start.1 = ((bf16[8,128,2048]{2,1,0:T(8,128)(2,1)}), bf16[8,128,2048]{2,1,0:T(8,128)(2,1)}, u32[]{:S(2)}, u32[]{:S(2)}) async-start(bf16[8,128,2048]{2,1,0:T(8,128)(2,1)} %stack.12), calls=%async_computation.1 | async-start | bytes 8388608 | tf_op jit(solution)/shard_map/all_to_all | solution.py:95
  20.0 0.7 copy-start.7
  20.0 1.4 copy-start.2
  20.0 1.4 copy-start.8
  20.0 206.8 %reduce-scatter.5.cloned.1.call-start = ((), (), s32[]{:S(2)}) async-start(), calls=%async_computation.6 | async-start | bytes 12976128 | tf_op jit(solution)/shard_map/reduce_scatter | solution.py:33
  20.1 1.8 copy-start.3
  68.4 8.4 %copy-start.1 = (f32[1024,704]{0,1:T(8,128)S(1)}, f32[1024,704]{0,1:T(8,128)}, u32[]{:S(2)}) copy-start(f32[1024,704]{0,1:T(8,128)} %get-tuple-element.33) | copy-start | bytes 8650756
  68.4 8.4 %copy-start.4 = (bf16[1024,704]{0,1:T(8,128)(2,1)S(1)}, bf16[1024,704]{0,1:T(8,128)(2,1)}, u32[]{:S(2)}) copy-start(bf16[1024,704]{0,1:T(8,128)(2,1)} %param.15) | copy-start | bytes 4325380
  96.0 28.7 %all-to-all-start.2 = ((f32[32,4,704]{2,1,0:T(4,128)}), f32[32,4,704]{2,1,0:T(4,128)S(1)}, u32[]{:S(2)}, u32[]{:S(2)}) async-start(f32[32,4,704]{2,1,0:T(4,128)} %broadcast_in_dim.2), calls=%async_computation.3 | async-start | bytes 786432 | tf_op jit(solution)/shard_map/all_to_all | solution.py:13
  105.8 7.0 %copy-start.5 = (bf16[1024,704]{0,1:T(8,128)(2,1)S(1)}, bf16[1024,704]{0,1:T(8,128)(2,1)}, u32[]{:S(2)}) copy-start(bf16[1024,704]{0,1:T(8,128)(2,1)} %param.15) | copy-start | bytes 4325380
  105.8 7.0 %copy-start.9 = (bf16[2048,1408]{1,0:T(8,128)(2,1)S(1)}, bf16[2048,1408]{1,0:T(8,128)(2,1)}, u32[]{:S(2)}) copy-start(bf16[2048,1408]{1,0:T(8,128)(2,1)} %all-gather.2.cloned.1.call-done) | copy-start | bytes 17301508
  124.7 105.8 %all-to-all-start = ((bf16[8,128,2048]{2,1,0:T(8,128)(2,1)}), bf16[8,128,2048]{2,1,0:T(8,128)(2,1)}, u32[]{:S(2)}, u32[]{:S(2)}) async-start(bf16[8,128,2048]{2,1,0:T(8,128)(2,1)} %bitcast.12), calls=%async_computation | async-start | bytes 8388608 | tf_op jit(solution)/shard_map/all_to_all | solution.py:45
  131.2 124.1 %reduce-scatter.7.cloned.1.call-start = ((), (), s32[]{:S(2)}) async-start(), calls=%async_computation.7 | async-start | bytes 1802240
  229.9 26.8 %copy-start.6 = (f32[4,704]{1,0:T(4,128)}, f32[4,704]{1,0:T(4,128)S(1)}, u32[]{:S(2)}) copy-start(f32[4,704]{1,0:T(4,128)S(1)} %broadcast_multiply_fusion.2) | copy-start | bytes 33796
Sparse Core Ops, SparseCore 0:
  12.0 89.4 all-gather.1
Sparse Core Ops, SparseCore 1:
  95.2 131.5 reduce-scatter.4
  229.9 25.4 reduce-scatter.6
